TPU v7x, 32 devices: a whole 2x2x4 slice. The times are simulated.
32 devices in a mesh: sp: 8 (over z, y), tp: 4 (over x, core).
Axes of the slice: x: 2, y: 2, z: 4, core: 2. Of those that a mesh axis runs over, the one named last changes fastest.
Arguments:
- stream: bfloat16 [3072, 2048], P(('sp', 'tp')), may hold values from -6 to 6
- query_projected: bfloat16 [3072, 1024], P('sp', 'tp'), may hold values from -6 to 6
- key_projected: bfloat16 [3072, 1024], P('sp', 'tp'), may hold values from -6 to 6
- value_projected: bfloat16 [3072, 1024], P('sp', 'tp'), may hold values from -6 to 6
- gate_projected: bfloat16 [3072, 1024], P('sp', 'tp'), may hold values from -6 to 6
- strength_logits: bfloat16 [8, 3072], P('tp', 'sp'), may hold values from -7 to 4
- decay_preactivation: bfloat16 [8, 3072], P('tp', 'sp'), may hold values from -9 to 9
- extra_log_decay: float32 [8, 3072], P('tp', 'sp'), may hold values from -0.7 to 0
- head_decay_rate: float32 [8], P('tp'), may hold values from 0 to 0.1
- head_norm_gain: float32 [128], replicated, may hold values from 0.1 to 1.9
- head_output_matrix: bfloat16 [1024, 2048], P('tp'), may hold values from -0.1875 to 0.1875
- feed_norm_gain: float32 [2048], replicated, may hold values from 0.1 to 1.9
- gate_matrix: bfloat16 [2048, 5632], P('sp', 'tp'), may hold values from -0.125 to 0.125
- up_matrix: bfloat16 [2048, 5632], P('sp', 'tp'), may hold values from -0.125 to 0.125
- down_matrix: bfloat16 [5632, 2048], P('tp', 'sp'), may hold values from -0.078125 to 0.078125
Outputs:
- result: bfloat16 [3072, 2048], P(('sp', 'tp'))
All inputs are finite; a program needn't handle non-finite values.
Results may differ from a plain program's by a relative error of at most 0.015.
Values may be sent and summed in bfloat16 or wider, within the bound.
No kernel may reach another device: no remote copies, remote signals or barrier semaphores. Data moves between devices by JAX's collectives and lax.ppermute only.
A program may use at most 128 MiB of HBM per device.

v0:
```python
import jax
import jax.numpy as jnp
from jax import lax
from jax.sharding import PartitionSpec as P

HEAD = 128
BLOCK = 64
PRECISION_FULL = lax.Precision.HIGHEST
EPSILON = 1e-06


def from_behind(value, axis, by):
    size = lax.axis_size(axis)
    pairs = [(i, i + by) for i in range(size) if 0 <= i + by < size]
    return lax.ppermute(value, axis, pairs)


def unit_rows(tensor):
    return tensor * lax.rsqrt(jnp.sum(tensor * tensor, axis=-1, keepdims=True) + EPSILON)


def rms_scale(tensor):
    return tensor * lax.rsqrt(jnp.mean(tensor * tensor, axis=-1, keepdims=True) + EPSILON)


def block_correction(
    unit_queries,
    unit_keys,
    complete_values,
    strength_logits,
    decay_preactivation,
    extra_log_decay,
    head_decay_rate,
):
    head_count, length, head_width = unit_queries.shape
    block_count = length // BLOCK

    def to_blocks(tensor):
        return tensor.reshape((head_count, block_count, BLOCK) + tensor.shape[2:])

    beta_gate = jax.nn.sigmoid(strength_logits.astype(jnp.float32))
    decay_logarithm = (
        -head_decay_rate[:, None] * jax.nn.softplus(decay_preactivation.astype(jnp.float32))
        + extra_log_decay
    )
    query_block = to_blocks(unit_queries)
    key_block = to_blocks(unit_keys)
    value_block = to_blocks(complete_values)
    beta_block = to_blocks(beta_gate)
    cumulative = jnp.cumsum(to_blocks(decay_logarithm), axis=-1)
    causal = jnp.tril(jnp.ones((BLOCK, BLOCK), bool))
    strict = jnp.tril(jnp.ones((BLOCK, BLOCK), bool), -1)
    spread = cumulative[..., :, None] - cumulative[..., None, :]
    damping = jnp.where(causal, jnp.exp(jnp.where(causal, spread, 0.0)), 0.0)
    key_beta = key_block * beta_block[..., None]
    lower_part = jnp.einsum(
        "hnid,hnjd->hnij", key_beta, key_block, precision=PRECISION_FULL
    ) * jnp.where(strict, damping, 0.0)
    system = lower_part + jnp.eye(BLOCK, dtype=jnp.float32)
    right_side = jnp.concatenate(
        [value_block * beta_block[..., None], key_beta * jnp.exp(cumulative)[..., None]], axis=-1
    )
    solved = lax.linalg.triangular_solve(
        system, right_side, left_side=True, lower=True, unit_diagonal=True
    )
    target_values = solved[..., :head_width]
    householder_weights = solved[..., head_width:]
    inner_scores = (
        jnp.einsum("hnid,hnjd->hnij", query_block, key_block, precision=PRECISION_FULL) * damping
    )
    decayed_queries = query_block * jnp.exp(cumulative)[..., None]
    closing_log_decay = cumulative[..., -1:]
    decayed_keys = key_block * jnp.exp(closing_log_decay - cumulative)[..., None]
    return (
        decayed_queries,
        decayed_keys,
        target_values,
        householder_weights,
        inner_scores,
        closing_log_decay,
    )


def local_recurrence(
    query_projected,
    key_projected,
    value_projected,
    strength_logits,
    decay_preactivation,
    extra_log_decay,
    head_decay_rate,
):
    head_count = strength_logits.shape[0]
    tok_count = strength_logits.shape[1]

    def split_heads(tensor):
        return tensor.reshape(tok_count, head_count, HEAD).transpose(1, 0, 2).astype(jnp.float32)

    unit_queries = unit_rows(split_heads(query_projected)) * HEAD ** (-0.5)
    unit_keys = unit_rows(split_heads(key_projected))
    complete_values = split_heads(value_projected)
    score_terms = block_correction(
        unit_queries,
        unit_keys,
        complete_values,
        strength_logits,
        decay_preactivation,
        extra_log_decay,
        head_decay_rate,
    )
    identity = jnp.broadcast_to(jnp.eye(HEAD, dtype=jnp.float32), (head_count, HEAD, HEAD))

    def advance(carry, items):
        running_state, matrix_product = carry
        (
            decayed_queries,
            decayed_keys,
            target_values,
            householder_weights,
            inner_scores,
            closing_log_decay,
        ) = items
        new_state = target_values - jnp.einsum(
            "fdc,fcj->fdj", householder_weights, running_state, precision=PRECISION_FULL
        )
        layer_output = jnp.einsum(
            "fdc,fcj->fdj", decayed_queries, running_state, precision=PRECISION_FULL
        )
        layer_output = layer_output + jnp.einsum(
            "hij,hjv->hiv", inner_scores, new_state, precision=PRECISION_FULL
        )
        passed_state = decayed_queries - jnp.einsum(
            "hij,hjk->hik", inner_scores, householder_weights, precision=PRECISION_FULL
        )
        decay_span = jnp.einsum(
            "fdc,fcj->fdj", passed_state, matrix_product, precision=PRECISION_FULL
        )
        decay_factor = jnp.exp(closing_log_decay)[:, :, None]
        step_map = decay_factor * identity - jnp.einsum(
            "hik,hij->hkj", decayed_keys, householder_weights, precision=PRECISION_FULL
        )
        running_state = decay_factor * running_state + jnp.einsum(
            "xwp,xws->xps", decayed_keys, new_state, precision=PRECISION_FULL
        )
        matrix_product = jnp.einsum(
            "hij,hjk->hik", step_map, matrix_product, precision=PRECISION_FULL
        )
        return ((running_state, matrix_product), (layer_output, decay_span))

    moved = tuple((jnp.moveaxis(tensor, 1, 0) for tensor in score_terms))
    zeros_state = jnp.zeros((head_count, HEAD, HEAD), jnp.float32)
    (running_state, matrix_product), (block_outputs, decay_spans) = lax.scan(
        advance, (zeros_state, identity), moved
    )

    def merge_blocks(tensor):
        return jnp.moveaxis(tensor, 0, 1).reshape(head_count, tok_count, HEAD)

    return (
        merge_blocks(block_outputs),
        merge_blocks(decay_spans),
        matrix_product,
        running_state,
        identity,
    )


def feed_forward(whole_rows, gate_matrix, up_matrix, down_matrix):
    gate_whole, up_whole = (
        lax.all_gather(gate_matrix, "sp", axis=0, tiled=True),
        lax.all_gather(up_matrix, "sp", axis=0, tiled=True),
    )
    gate_total = jnp.dot(whole_rows, gate_whole, preferred_element_type=jnp.float32)
    up_total = jnp.dot(whole_rows, up_whole, preferred_element_type=jnp.float32)
    hidden = (jax.nn.silu(gate_total) * up_total).astype(jnp.bfloat16)
    down_whole = lax.all_gather(down_matrix, "sp", axis=1, tiled=True)
    return jnp.dot(hidden, down_whole, preferred_element_type=jnp.float32)


def body(
    stream,
    query_projected,
    key_projected,
    value_projected,
    gate_projected,
    strength_logits,
    decay_preactivation,
    extra_log_decay,
    head_decay_rate,
    head_norm_gain,
    head_output_matrix,
    feed_norm_gain,
    gate_matrix,
    up_matrix,
    down_matrix,
):
    block_outputs, decay_spans, matrix_product, running_state, identity = local_recurrence(
        query_projected,
        key_projected,
        value_projected,
        strength_logits,
        decay_preactivation,
        extra_log_decay,
        head_decay_rate,
    )
    zeros_state = jnp.zeros_like(running_state)

    def pass_state(turn, state_inflow):
        leaving = (
            jnp.einsum("hij,hjk->hik", matrix_product, state_inflow, precision=PRECISION_FULL)
            + running_state
        )
        return from_behind(leaving.astype(jnp.bfloat16), "sp", 1).astype(leaving.dtype)

    state_inflow = lax.fori_loop(0, lax.axis_size("sp") - 1, pass_state, zeros_state)
    attention_output = block_outputs + jnp.einsum(
        "qwc,qcn->qwn", decay_spans, state_inflow, precision=PRECISION_FULL
    )
    head_count = attention_output.shape[0]
    tok_count = attention_output.shape[1]
    normed_heads = rms_scale(attention_output) * head_norm_gain
    gated = normed_heads.transpose(1, 0, 2).reshape(tok_count, head_count * HEAD)
    mixed = (gated * jax.nn.silu(gate_projected.astype(jnp.float32))).astype(jnp.bfloat16)
    branch = lax.psum_scatter(
        jnp.dot(mixed, head_output_matrix, preferred_element_type=jnp.float32).astype(jnp.bfloat16),
        "tp",
        scatter_dimension=0,
        tiled=True,
    ).astype(jnp.float32)
    residual_own = stream.astype(jnp.float32) + branch
    normed_own = (rms_scale(residual_own) * feed_norm_gain).astype(jnp.bfloat16)
    whole_rows = lax.all_gather(normed_own, "tp", axis=0, tiled=True)
    ffn_term = feed_forward(whole_rows, gate_matrix, up_matrix, down_matrix)
    ffn_own = lax.psum_scatter(
        ffn_term.astype(jnp.bfloat16), "tp", scatter_dimension=0, tiled=True
    ).astype(jnp.float32)
    return (residual_own + ffn_own).astype(jnp.bfloat16)


def solution(mesh):
    placed = (
        P(("sp", "tp"), None),
        P("sp", "tp"),
        P("sp", "tp"),
        P("sp", "tp"),
        P("sp", "tp"),
        P("tp", "sp"),
        P("tp", "sp"),
        P("tp", "sp"),
        P("tp"),
        P(),
        P("tp", None),
        P(),
        P("sp", "tp"),
        P("sp", "tp"),
        P("tp", "sp"),
    )
    return jax.shard_map(
        body, mesh=mesh, in_specs=placed, out_specs=P(("sp", "tp"), None), check_vma=False
    )
```

profile of v0, /device:TPU:0, one launch (start us, length us, event | category | flops | bytes accessed | tf_op | source)
XLA Modules:
  0.0 551.2 jit_solution(7347479485389619198)
XLA Ops:
  8.9 1.1 fusion.64
  10.0 1.1 fusion.62
  11.1 1.1 fusion.60
  12.2 1.1 fusion.61
  14.1 1.0 copy_bitcast_fusion
  16.0 59.6 %custom-call.3 = f32[2,6,1,64,64]{3,4,2,1,0:T(8,128)} custom-call(f32[2,6,1,64,64]{4,3,2,1,0:T(8,128)S(1)} %fusion.48), custom_call_target="InvertDiagBlocksLowerTriangular" | custom-call | tf_op jit(solution)/shard_map/triangular_solve | solution.py:63
  75.6 1.1 multiply_multiply_fusion
  76.7 0.9 fusion.49
  77.6 0.8 slice_bitcast_fusion
  79.3 36.4 %while.28 = (s32[]{:T(128)}, f32[2,128,128]{2,1,0:T(8,128)S(1)}, f32[2,128,128]{2,1,0:T(8,128)S(1)}, f32[6,2,64,128]{3,2,0,1:T(8,128)}, f32[6,2,64,128]{3,2,0,1:...) while((s32[]{:T(128)}, f32[2,128,128]{2,1,0:T(8,128)S(1)}, ...), condition=%wide.region_4.5_spmd.clone, body=%wide.region_3.4_spmd.clone.sunk | while | flops 201605120 | bytes 2759337 | solution.py:152
  79.4 1.1 convolution_subtract_fusion.6
  80.5 1.1 fusion.145
  81.5 0.8 fusion.146
  82.8 1.0 convolution_subtract_fusion.8
  83.9 0.9 fusion.147
  85.4 1.1 convolution_subtract_fusion.6
  86.5 1.1 fusion.145
  87.6 0.8 fusion.146
  88.9 1.0 convolution_subtract_fusion.8
  89.9 0.9 fusion.147
  91.5 1.1 convolution_subtract_fusion.6
  92.6 1.1 fusion.145
  94.9 1.0 convolution_subtract_fusion.8
  96.0 0.9 fusion.147
  97.5 1.1 convolution_subtract_fusion.6
  98.6 1.1 fusion.145
  101.0 1.0 convolution_subtract_fusion.8
  102.0 0.9 fusion.147
  103.6 1.1 convolution_subtract_fusion.6
  104.7 1.1 fusion.145
  107.0 1.0 convolution_subtract_fusion.8
  108.1 0.9 fusion.147
  109.7 1.1 convolution_subtract_fusion.6
  110.7 1.1 fusion.145
  113.1 1.0 convolution_subtract_fusion.8
  114.2 0.9 fusion.147
  115.7 1.2 copy.42
  116.9 49.8 %while.29 = (s32[]{:T(128)}, f32[2,128,128]{2,1,0:T(8,128)S(1)}, f32[2,128,128]{2,1,0:T(8,128)S(1)}, f32[2,128,128]{2,1,0:T(8,128)S(1)}, s32[]{:T(128)}, /*index=5*/s32[]{:T(128)}) while((s32[]{:T(128)}, f32[2,128,128]{2,1,0:T(8,128)S(1)}, f32[2,128,128]{2,1,0:T(8,128)S(1)}, f32[2,128,128]{2,1,0:T(8,128)S(1)}, s32[]{:T(128)}, ...), condition=%wide.region_6.7_spmd.clone, body=%wide.region_5.6_spmd.clone.sunk | while | flops 50462720 | bytes 917623 | solution.py:215
  117.2 4.9 collective-permute-start
  122.1 1.9 collective-permute-done
  124.3 4.3 collective-permute-start
  128.6 1.9 collective-permute-done
  130.8 4.3 collective-permute-start
  135.1 1.9 collective-permute-done
  137.3 5.2 collective-permute-start
  142.5 1.9 collective-permute-done
  144.7 5.2 collective-permute-start
  149.9 1.9 collective-permute-done
  152.1 5.3 collective-permute-start
  157.3 2.1 collective-permute-done
  159.7 5.1 collective-permute-start
  164.8 1.9 collective-permute-done
  167.8 1.8 convolution_convert_fusion.1
  169.6 31.9 %reduce-scatter.3.cloned.1.call-done = bf16[96,2048]{1,0:T(8,128)(2,1)} async-done(((bf16[384,2048]{1,0:T(8,128)(2,1)}), bf16[96,2048]{1,0:T(8,128)(2,1)}) %reduce-scatter.3.cloned.1.call-update) | async-done | bytes 393232 | tf_op jit(solution)/shard_map/reduce_scatter | solution.py:224
  201.5 1.2 multiply_reduce_fusion
  202.8 1.9 multiply_convert_fusion
  206.8 17.7 %all-gather.5.cloned.1.call-done = bf16[384,2048]{1,0:T(8,128)(2,1)} async-done(((bf16[96,2048]{1,0:T(8,128)(2,1)}), bf16[384,2048]{1,0:T(8,128)(2,1)}) %all-gather.5.cloned.1.call-update) | async-done | bytes 1572880 | tf_op jit(solution)/shard_map/all_gather | solution.py:232
  224.5 94.5 %all-gather.7.cloned.1.call-done = bf16[2048,1408]{1,0:T(8,128)(2,1)} async-done(((bf16[256,1408]{1,0:T(8,128)(2,1)}), bf16[2048,1408]{1,0:T(8,128)(2,1)}) %all-gather.7.cloned.1.call-update) | async-done | bytes 5767184 | tf_op jit(solution)/shard_map/all_gather | solution.py:170
  319.0 7.1 %fusion.84 = f32[384,1408]{1,0:T(8,128)} fusion(bf16[384,2048]{1,0:T(8,128)(2,1)} %all-gather.5.cloned.1.call-done, bf16[2048,1408]{1,0:T(8,128)(2,1)} %all-gather.7.cloned.1.call-done), kind=kOutput, calls=%fused_computation.133 | convolution fusion | flops 2214592512 | bytes 9502720 | tf_op jit(solution)/shard_map/dot_general | solution.py:173
  326.1 86.2 %all-gather.11.cloned.1.call-done = bf16[1408,2048]{1,0:T(8,128)(2,1)} async-done(((bf16[1408,256]{1,0:T(8,128)(2,1)}), bf16[1408,2048]{1,0:T(8,128)(2,1)}) %all-gather.11.cloned.1.call-update) | async-done | bytes 5767184 | tf_op jit(solution)/shard_map/all_gather | solution.py:176
  412.3 92.6 %all-gather.9.cloned.1.call-done = bf16[2048,1408]{1,0:T(8,128)(2,1)} async-done(((bf16[256,1408]{1,0:T(8,128)(2,1)}), bf16[2048,1408]{1,0:T(8,128)(2,1)}) %all-gather.9.cloned.1.call-update) | async-done | bytes 5767184 | tf_op jit(solution)/shard_map/all_gather | solution.py:171
  504.8 11.3 %convolution_convert_fusion = bf16[384,2048]{1,0:T(8,128)(2,1)} fusion(bf16[1408,2048]{1,0:T(8,128)(2,1)} %all-gather.11.cloned.1.call-done, bf16[384,2048]{1,0:T(8,128)(2,1)S(1)} %copy-done.7, bf16[2048,1408]{1,0:T(8,128)(2,1)} %all-gather.9.cloned.1.call-done, f32[384,1408]{1,0:T(8,128)} %fusion.84), kind=kOutput, calls=%fused_computation.52 | convolution fusion | flops 4433215488 | bytes 16842752 | tf_op jit(solution)/shard_map/dot_general | solution.py:177
  516.1 26.4 %reduce-scatter.5.cloned.1.call-done = bf16[96,2048]{1,0:T(8,128)(2,1)} async-done(((bf16[384,2048]{1,0:T(8,128)(2,1)}), bf16[96,2048]{1,0:T(8,128)(2,1)}) %reduce-scatter.5.cloned.1.call-update) | async-done | bytes 393232 | tf_op jit(solution)/shard_map/reduce_scatter | solution.py:234
  542.5 1.9 add_convert_fusion
  (105 shorter events, 19.7 us)
Async XLA Ops:
  6.5 161.2 %copy-start = (bf16[256,2048]{1,0:T(8,128)(2,1)S(1)}, bf16[256,2048]{1,0:T(8,128)(2,1)}, u32[]{:S(2)}) copy-start(bf16[256,2048]{1,0:T(8,128)(2,1)} %param.29) | copy-start | bytes 3145732
  6.5 195.0 %reduce-scatter.3.cloned.1.call-start = ((), (), s32[]{:S(2)}) async-start(), calls=%async_computation.2 | async-start | bytes 1966080 | tf_op jit(solution)/shard_map/reduce_scatter | solution.py:224
  75.6 1.1 copy-start.4
  115.7 51.0 %copy-start.3 = (f32[6,2,64,128]{3,2,0,1:T(8,128)S(1)}, f32[6,2,64,128]{3,2,0,1:T(8,128)}, u32[]{:S(2)}) copy-start(f32[6,2,64,128]{3,2,0,1:T(8,128)} %get-tuple-element.93) | copy-start | bytes 1179652
  116.9 50.5 %copy-start.6 = (f32[128]{0:T(128)S(1)}, f32[128]{0:T(128)}, u32[]{:S(2)}) copy-start(f32[128]{0:T(128)} %param.28) | copy-start | bytes 1540
  117.2 6.8 %collective-permute-start = (bf16[2,128,128]{2,1,0:T(8,128)(2,1)S(1)}, bf16[2,128,128]{2,1,0:T(8,128)(2,1)S(1)}, u32[]{:S(2)}, u32[]{:S(2)}) collective-permute-start(bf16[2,128,128]{2,1,0:T(8,128)(2,1)S(1)} %fusion.150), channel_id=1, source_target_pairs={{0,4},{4,8},{8,12},{12,16},{16,20},{20,24},{24,28},{1,5},{5,9},{9,... | collective-permute-start | bytes 196616 | tf_op jit(solution)/shard_map/while/body/eval_jaxpr/ppermute | solution.py:15
  124.3 6.2 %collective-permute-start = (bf16[2,128,128]{2,1,0:T(8,128)(2,1)S(1)}, bf16[2,128,128]{2,1,0:T(8,128)(2,1)S(1)}, u32[]{:S(2)}, u32[]{:S(2)}) collective-permute-start(bf16[2,128,128]{2,1,0:T(8,128)(2,1)S(1)} %fusion.150), channel_id=1, source_target_pairs={{0,4},{4,8},{8,12},{12,16},{16,20},{20,24},{24,28},{1,5},{5,9},{9,... | collective-permute-start | bytes 196616 | tf_op jit(solution)/shard_map/while/body/eval_jaxpr/ppermute | solution.py:15
  130.8 6.2 %collective-permute-start = (bf16[2,128,128]{2,1,0:T(8,128)(2,1)S(1)}, bf16[2,128,128]{2,1,0:T(8,128)(2,1)S(1)}, u32[]{:S(2)}, u32[]{:S(2)}) collective-permute-start(bf16[2,128,128]{2,1,0:T(8,128)(2,1)S(1)} %fusion.150), channel_id=1, source_target_pairs={{0,4},{4,8},{8,12},{12,16},{16,20},{20,24},{24,28},{1,5},{5,9},{9,... | collective-permute-start | bytes 196616 | tf_op jit(solution)/shard_map/while/body/eval_jaxpr/ppermute | solution.py:15
  137.3 7.1 %collective-permute-start = (bf16[2,128,128]{2,1,0:T(8,128)(2,1)S(1)}, bf16[2,128,128]{2,1,0:T(8,128)(2,1)S(1)}, u32[]{:S(2)}, u32[]{:S(2)}) collective-permute-start(bf16[2,128,128]{2,1,0:T(8,128)(2,1)S(1)} %fusion.150), channel_id=1, source_target_pairs={{0,4},{4,8},{8,12},{12,16},{16,20},{20,24},{24,28},{1,5},{5,9},{9,... | collective-permute-start | bytes 196616 | tf_op jit(solution)/shard_map/while/body/eval_jaxpr/ppermute | solution.py:15
  144.7 7.1 %collective-permute-start = (bf16[2,128,128]{2,1,0:T(8,128)(2,1)S(1)}, bf16[2,128,128]{2,1,0:T(8,128)(2,1)S(1)}, u32[]{:S(2)}, u32[]{:S(2)}) collective-permute-start(bf16[2,128,128]{2,1,0:T(8,128)(2,1)S(1)} %fusion.150), channel_id=1, source_target_pairs={{0,4},{4,8},{8,12},{12,16},{16,20},{20,24},{24,28},{1,5},{5,9},{9,... | collective-permute-start | bytes 196616 | tf_op jit(solution)/shard_map/while/body/eval_jaxpr/ppermute | solution.py:15
  152.1 7.4 %collective-permute-start = (bf16[2,128,128]{2,1,0:T(8,128)(2,1)S(1)}, bf16[2,128,128]{2,1,0:T(8,128)(2,1)S(1)}, u32[]{:S(2)}, u32[]{:S(2)}) collective-permute-start(bf16[2,128,128]{2,1,0:T(8,128)(2,1)S(1)} %fusion.150), channel_id=1, source_target_pairs={{0,4},{4,8},{8,12},{12,16},{16,20},{20,24},{24,28},{1,5},{5,9},{9,... | collective-permute-start | bytes 196616 | tf_op jit(solution)/shard_map/while/body/eval_jaxpr/ppermute | solution.py:15
  159.7 7.0 %collective-permute-start = (bf16[2,128,128]{2,1,0:T(8,128)(2,1)S(1)}, bf16[2,128,128]{2,1,0:T(8,128)(2,1)S(1)}, u32[]{:S(2)}, u32[]{:S(2)}) collective-permute-start(bf16[2,128,128]{2,1,0:T(8,128)(2,1)S(1)} %fusion.150), channel_id=1, source_target_pairs={{0,4},{4,8},{8,12},{12,16},{16,20},{20,24},{24,28},{1,5},{5,9},{9,... | collective-permute-start | bytes 196616 | tf_op jit(solution)/shard_map/while/body/eval_jaxpr/ppermute | solution.py:15
  166.7 1.0 copy-start.8
  167.7 33.8 %copy-start.1 = (bf16[96,2048]{1,0:T(8,128)(2,1)S(1)}, bf16[96,2048]{1,0:T(8,128)(2,1)}, u32[]{:S(2)}) copy-start(bf16[96,2048]{1,0:T(8,128)(2,1)} %param.19) | copy-start | bytes 1179652
  167.7 35.0 %copy-start.5 = (f32[2048]{0:T(1024)S(1)}, f32[2048]{0:T(1024)}, u32[]{:S(2)}) copy-start(f32[2048]{0:T(1024)} %param.30) | copy-start | bytes 24580
  169.6 54.9 %all-gather.5.cloned.1.call-start = ((), (), s32[]{:S(2)}) async-start(), calls=%async_computation.3 | async-start | bytes 1966080 | tf_op jit(solution)/shard_map/all_gather | solution.py:232
  204.7 114.3 %all-gather.7.cloned.1.call-start = ((), (), s32[]{:S(2)}) async-start(), calls=%async_computation.4 | async-start | bytes 6488064 | tf_op jit(solution)/shard_map/all_gather | solution.py:170
  205.4 206.8 %all-gather.11.cloned.1.call-start = ((), (), s32[]{:S(2)}) async-start(), calls=%async_computation.6 | async-start | bytes 6488064 | tf_op jit(solution)/shard_map/all_gather | solution.py:176
  206.0 298.8 %all-gather.9.cloned.1.call-start = ((), (), s32[]{:S(2)}) async-start(), calls=%async_computation.5 | async-start | bytes 6488064 | tf_op jit(solution)/shard_map/all_gather | solution.py:171
  206.6 335.9 %reduce-scatter.5.cloned.1.call-start = ((), (), s32[]{:S(2)}) async-start(), calls=%async_computation.7 | async-start | bytes 1966080 | tf_op jit(solution)/shard_map/reduce_scatter | solution.py:234
  224.5 280.3 %copy-start.7 = (bf16[384,2048]{1,0:T(8,128)(2,1)S(1)}, bf16[384,2048]{1,0:T(8,128)(2,1)}, u32[]{:S(2)}) copy-start(bf16[384,2048]{1,0:T(8,128)(2,1)} %all-gather.5.cloned.1.call-done) | copy-start | bytes 4718596
  326.1 216.4 %copy-start.2 = (bf16[96,2048]{1,0:T(8,128)(2,1)S(1)}, bf16[96,2048]{1,0:T(8,128)(2,1)}, u32[]{:S(2)}) copy-start(bf16[96,2048]{1,0:T(8,128)(2,1)} %reduce-scatter.3.cloned.1.call-done) | copy-start | bytes 1179652
Sparse Core Ops, SparseCore 0:
  169.7 31.7 reduce-scatter.2
  204.8 19.6 all-gather.4
  226.7 92.3 all-gather.6
  320.9 91.2 all-gather.10
  414.3 90.4 all-gather.8
  516.2 26.1 reduce-scatter.4
where the time goes:
time: 553 us; the launch traced here: 551 us
  waiting for transfers between devices  364 us (66%)
  other arithmetic  74.1 us (13%)
  matrix products  60.9 us (11%)
  starting transfers between devices  34.5 us (6%)
  between operations  13.7 us (2%)
    all_gather x1, waiting for transfers between devices, feed_forward(): lax.all_gather(gate_matrix, 'sp', axis=0, tiled=True)  94.5 us
    all_gather x1, waiting for transfers between devices, feed_forward(): lax.all_gather(up_matrix, 'sp', axis=0, tiled=True)  92.6 us
    all_gather x1, waiting for transfers between devices, feed_forward(): down_whole = lax.all_gather(down_matrix, 'sp', axis=1, tiled=True)  86.2 us
    another operation x2, other arithmetic, block_correction(): lax.linalg.triangular_solve(system, right_side, left_side=True, lower=Tru...  59.6 us
    ppermute x7, starting transfers between devices, from_behind(): return lax.ppermute(value, axis, pairs)  34.2 us
    reduce_scatter x1, waiting for transfers between devices, body(): lax.psum_scatter(jnp.dot(mixed, head_output_matrix, preferred_element_typ...  31.9 us
    reduce_scatter x1, waiting for transfers between devices, body(): lax.psum_scatter(ffn_term.astype(jnp.bfloat16), 'tp', scatter_dimension=0...  26.4 us
    all_gather x1, waiting for transfers between devices, body(): whole_rows = lax.all_gather(normed_own, 'tp', axis=0, tiled=True)  17.7 us
  transfers between devices with their start and end apart: 13, of which 13 were waited for; matrix products, arithmetic and copies ran while one was open for 1% of the time, Pallas kernels for 0%

commit v1 on v0

--- a/solution.py
+++ b/solution.py
@@ -173,7 +173,14 @@
     gate_total = jnp.dot(whole_rows, gate_whole, preferred_element_type=jnp.float32)
     up_total = jnp.dot(whole_rows, up_whole, preferred_element_type=jnp.float32)
     hidden = (jax.nn.silu(gate_total) * up_total).astype(jnp.bfloat16)
-    down_whole = lax.all_gather(down_matrix, "sp", axis=1, tiled=True)
+    count = lax.axis_size("sp")
+    forward = [(i_2, (i_2 + 1) % count) for i_2 in range(count)]
+    shards = [down_matrix]
+    for hop in range(1, count):
+        shards = [lax.ppermute(shards[0], "sp", forward), *shards]
+    out = jnp.concatenate(shards, axis=1)
+    places = (lax.axis_index("sp") + 1) * shards[-1].shape[1]
+    down_whole = jnp.roll(out, places, axis=1)
     return jnp.dot(hidden, down_whole, preferred_element_type=jnp.float32)
 
 

time: 553 us -> 534 us (0.966)
  waiting for transfers between devices: 364 us -> 307 us
  local copies, waits for them, and re-layouts: 2.78 us -> 31 us
  matrix products: 60.9 us -> 70.4 us
    ppermute x0 -> x7, waiting for transfers between devices: none -> 202 us  [feed_forward(): shards = [lax.ppermute(shards[0], 'sp', forward), *shards]]
    all_gather x1, waiting for transfers between devices: 94.5 us -> 0.01 us  [feed_forward(): lax.all_gather(gate_matrix, 'sp', axis=0, tiled=True)]
    all_gather x1 -> x0, waiting for transfers between devices: 86.2 us -> none  [feed_forward(): down_whole = lax.all_gather(down_matrix, 'sp', axis=1, tiled=True)]
    all_gather x1, waiting for transfers between devices: 92.6 us -> 31.6 us  [feed_forward(): lax.all_gather(up_matrix, 'sp', axis=0, tiled=True)]
    unnamed x19 -> x44, local copies, waits for them, and re-layouts: 0.17 us -> 27.5 us
    all_gather x1, waiting for transfers between devices: 17.7 us -> 0.01 us  [body(): whole_rows = lax.all_gather(normed_own, 'tp', axis=0, tiled=True)]
  transfers between devices with their start and end apart: 13 -> 19, of which waited for: 13 -> 17; matrix products, arithmetic and copies ran while one was open for 1% -> 6% of each run, Pallas kernels for 0% -> 0%
where the time goes in v1:
time: 534 us; the launch traced here: 532 us
  waiting for transfers between devices  307 us (57%)
  other arithmetic  74.1 us (14%)
  matrix products  70.4 us (13%)
  starting transfers between devices  35.9 us (7%)
  local copies, waits for them, and re-layouts  31 us (6%)
  between operations  13.4 us (3%)
    ppermute x7, waiting for transfers between devices, feed_forward(): shards = [lax.ppermute(shards[0], 'sp', forward), *shards]  202 us
    another operation x2, other arithmetic, block_correction(): lax.linalg.triangular_solve(system, right_side, left_side=True, lower=Tru...  59.6 us
    ppermute x7, starting transfers between devices, from_behind(): return lax.ppermute(value, axis, pairs)  34.2 us
    reduce_scatter x1, waiting for transfers between devices, body(): lax.psum_scatter(jnp.dot(mixed, head_output_matrix, preferred_element_typ...  31.9 us
    all_gather x1, waiting for transfers between devices, feed_forward(): lax.all_gather(up_matrix, 'sp', axis=0, tiled=True)  31.6 us
    unnamed x44, local copies, waits for them, and re-layouts  27.5 us
    reduce_scatter x1, waiting for transfers between devices, body(): lax.psum_scatter(ffn_term.astype(jnp.bfloat16), 'tp', scatter_dimension=0...  26.4 us
    ppermute x7, waiting for transfers between devices, from_behind(): return lax.ppermute(value, axis, pairs)  13.4 us
  transfers between devices with their start and end apart: 19, of which 17 were waited for; matrix products, arithmetic and copies ran while one was open for 6% of the time, Pallas kernels for 0%

profile of v1, /device:TPU:0, one launch (start us, length us, event | category | flops | bytes accessed | tf_op | source)
XLA Modules:
  0.0 532.2 jit_solution(2902205664689989090)
XLA Ops:
  8.9 1.1 fusion.69
  10.0 1.1 fusion.67
  12.0 1.1 fusion.65
  13.1 1.1 fusion.66
  16.1 59.6 %custom-call.3 = f32[2,6,1,64,64]{3,4,2,1,0:T(8,128)} custom-call(f32[2,6,1,64,64]{4,3,2,1,0:T(8,128)S(1)} %fusion.53), custom_call_target="InvertDiagBlocksLowerTriangular" | custom-call | tf_op jit(solution)/shard_map/triangular_solve | solution.py:63
  75.7 1.1 multiply_multiply_fusion
  76.8 1.8 fusion.54
  79.5 1.5 fusion.49
  81.1 41.8 %while.28 = (s32[]{:T(128)}, f32[2,128,128]{2,1,0:T(8,128)S(1)}, f32[2,128,128]{2,1,0:T(8,128)S(1)}, f32[6,2,64,128]{3,2,0,1:T(8,128)}, f32[6,2,64,128]{3,2,0,1:...) while((s32[]{:T(128)}, f32[2,128,128]{2,1,0:T(8,128)S(1)}, ...), condition=%wide.region_4.5_spmd.clone, body=%wide.region_3.4_spmd.clone.sunk | while | flops 201605120 | bytes 2758840 | solution.py:152
  81.1 1.2 fusion.150
  82.3 1.1 convolution_subtract_fusion.6
  86.5 1.7 fusion.151
  89.2 1.1 convolution_subtract_fusion.6
  93.4 1.7 fusion.151
  96.2 1.1 convolution_subtract_fusion.6
  100.4 1.7 fusion.151
  103.1 1.1 convolution_subtract_fusion.6
  107.3 1.7 fusion.151
  110.1 1.1 convolution_subtract_fusion.6
  114.2 1.7 fusion.151
  117.0 1.1 convolution_subtract_fusion.6
  121.2 1.7 fusion.151
  122.9 1.2 copy.42
  124.0 49.8 %while.29 = (s32[]{:T(128)}, f32[2,128,128]{2,1,0:T(8,128)S(1)}, f32[2,128,128]{2,1,0:T(8,128)S(1)}, f32[2,128,128]{2,1,0:T(8,128)S(1)}, s32[]{:T(128)}, /*index=5*/s32[]{:T(128)}) while((s32[]{:T(128)}, f32[2,128,128]{2,1,0:T(8,128)S(1)}, f32[2,128,128]{2,1,0:T(8,128)S(1)}, f32[2,128,128]{2,1,0:T(8,128)S(1)}, s32[]{:T(128)}, ...), condition=%wide.region_6.7_spmd.clone, body=%wide.region_5.6_spmd.clone.sunk | while | flops 50462720 | bytes 917623 | solution.py:222
  124.3 4.9 collective-permute-start
  129.2 1.9 collective-permute-done
  131.4 4.3 collective-permute-start
  135.7 1.9 collective-permute-done
  137.9 4.3 collective-permute-start
  142.2 1.9 collective-permute-done
  144.4 5.2 collective-permute-start
  149.6 1.9 collective-permute-done
  151.8 5.2 collective-permute-start
  157.0 1.9 collective-permute-done
  159.1 5.3 collective-permute-start
  164.4 2.1 collective-permute-done
  166.8 5.1 collective-permute-start
  171.9 1.9 collective-permute-done
  173.8 1.7 multiply_reduce_fusion.1
  175.8 2.7 convolution_convert_fusion
  178.6 31.9 %reduce-scatter.3.cloned.1.call-done = bf16[96,2048]{1,0:T(8,128)(2,1)} async-done(((bf16[384,2048]{1,0:T(8,128)(2,1)}), bf16[96,2048]{1,0:T(8,128)(2,1)}) %reduce-scatter.3.cloned.1.call-update) | async-done | bytes 393232 | tf_op jit(solution)/shard_map/reduce_scatter | solution.py:231
  210.4 1.2 multiply_reduce_fusion
  211.7 1.9 multiply_convert_fusion
  215.0 1.5 collective-permute-start.1
  216.5 18.9 %collective-permute-done.1 = bf16[1408,256]{1,0:T(8,128)(2,1)S(1)} collective-permute-done((bf16[1408,256]{1,0:T(8,128)(2,1)S(1)}, bf16[1408,256]{1,0:T(8,128)(2,1)S(1)}, u32[]{:S(2)}, u32[]{:S(2)}) %collective-permute-start.1) | collective-permute-done | bytes 720928 | tf_op jit(solution)/shard_map/ppermute | solution.py:180
  235.5 27.2 %collective-permute-done.2 = bf16[1408,256]{1,0:T(8,128)(2,1)S(1)} collective-permute-done((bf16[1408,256]{1,0:T(8,128)(2,1)S(1)}, bf16[1408,256]{1,0:T(8,128)(2,1)S(1)}, u32[]{:S(2)}, u32[]{:S(2)}) %collective-permute-start.2) | collective-permute-done | bytes 720928 | tf_op jit(solution)/shard_map/ppermute | solution.py:180
  263.5 30.2 %collective-permute-done.3 = bf16[1408,256]{1,0:T(8,128)(2,1)S(1)} collective-permute-done((bf16[1408,256]{1,0:T(8,128)(2,1)S(1)}, bf16[1408,256]{1,0:T(8,128)(2,1)S(1)}, u32[]{:S(2)}, u32[]{:S(2)}) %collective-permute-start.3) | collective-permute-done | bytes 720928 | tf_op jit(solution)/shard_map/ppermute | solution.py:180
  294.6 35.0 %collective-permute-done.4 = bf16[1408,256]{1,0:T(8,128)(2,1)S(1)} collective-permute-done((bf16[1408,256]{1,0:T(8,128)(2,1)S(1)}, bf16[1408,256]{1,0:T(8,128)(2,1)S(1)}, u32[]{:S(2)}, u32[]{:S(2)}) %collective-permute-start.4) | collective-permute-done | bytes 720928 | tf_op jit(solution)/shard_map/ppermute | solution.py:180
  330.5 35.1 %collective-permute-done.5 = bf16[1408,256]{1,0:T(8,128)(2,1)S(1)} collective-permute-done((bf16[1408,256]{1,0:T(8,128)(2,1)S(1)}, bf16[1408,256]{1,0:T(8,128)(2,1)S(1)}, u32[]{:S(2)}, u32[]{:S(2)}) %collective-permute-start.5) | collective-permute-done | bytes 720928 | tf_op jit(solution)/shard_map/ppermute | solution.py:180
  366.5 23.5 %collective-permute-done.6 = bf16[1408,256]{1,0:T(8,128)(2,1)} collective-permute-done((bf16[1408,256]{1,0:T(8,128)(2,1)S(1)}, bf16[1408,256]{1,0:T(8,128)(2,1)}, u32[]{:S(2)}, u32[]{:S(2)}) %collective-permute-start.6) | collective-permute-done | bytes 720928 | tf_op jit(solution)/shard_map/ppermute | solution.py:180
  390.1 32.3 %collective-permute-done.7 = bf16[1408,256]{1,0:T(8,128)(2,1)} collective-permute-done((bf16[1408,256]{1,0:T(8,128)(2,1)}, bf16[1408,256]{1,0:T(8,128)(2,1)}, u32[]{:S(2)}, u32[]{:S(2)}) %collective-permute-start.7) | collective-permute-done | bytes 720928 | tf_op jit(solution)/shard_map/ppermute | solution.py:180
  422.4 2.1 constant_dynamic-update-slice_fusion.15
  424.4 2.1 constant_dynamic-update-slice_fusion.14
  426.5 2.1 constant_dynamic-update-slice_fusion.13
  428.6 2.1 constant_dynamic-update-slice_fusion.12
  430.7 2.1 constant_dynamic-update-slice_fusion.11
  432.8 2.3 constant_dynamic-update-slice_fusion.10
  437.1 2.1 constant_dynamic-update-slice_fusion.7
  439.1 2.1 constant_dynamic-update-slice_fusion.6
  447.0 7.1 %fusion.90 = f32[384,1408]{1,0:T(8,128)} fusion(bf16[384,2048]{1,0:T(8,128)(2,1)} %all-gather.4.cloned.1.call-done, bf16[2048,1408]{1,0:T(8,128)(2,1)} %all-gather.6.cloned.1.call-done), kind=kOutput, calls=%fused_computation.152 | convolution fusion | flops 2214592512 | bytes 9502720 | tf_op jit(solution)/shard_map/dot_general | solution.py:173
  454.1 31.6 %all-gather.8.cloned.1.call-done = bf16[2048,1408]{1,0:T(8,128)(2,1)} async-done(((bf16[256,1408]{1,0:T(8,128)(2,1)}), bf16[2048,1408]{1,0:T(8,128)(2,1)}) %all-gather.8.cloned.1.call-update) | async-done | bytes 5767184 | tf_op jit(solution)/shard_map/all_gather | solution.py:171
  485.7 11.7 %fusion.46 = bf16[384,2048]{1,0:T(8,128)(2,1)} fusion(bf16[1408,4096]{1,0:T(8,128)(2,1)} %constant_dynamic-update-slice_fusion, s32[]{:T(128)S(6)} %select_n.44, bf16[384,2048]{1,0:T(8,128)(2,1)} %all-gather.4.cloned.1.call-done, bf16[2048,1408]{1,0:T(8,128)(2,1)} %all-gather.8.cloned.1.call-done, f32[384,1408]{1,0:T(8,128)} %fusion.90), kind=kOutput, calls=%fused_computation.54 | convolution fusion | flops 4433215488 | bytes 16842756 | tf_op jit(solution)/shard_map/dot_general | solution.py:184
  497.4 26.4 %reduce-scatter.5.cloned.1.call-done = bf16[96,2048]{1,0:T(8,128)(2,1)} async-done(((bf16[384,2048]{1,0:T(8,128)(2,1)}), bf16[96,2048]{1,0:T(8,128)(2,1)}) %reduce-scatter.5.cloned.1.call-update) | async-done | bytes 393232 | tf_op jit(solution)/shard_map/reduce_scatter | solution.py:241
  523.7 1.9 add_convert_fusion
  (142 shorter events, 44.5 us)
Async XLA Ops:
  6.5 169.2 %copy-start = (bf16[256,2048]{1,0:T(8,128)(2,1)S(1)}, bf16[256,2048]{1,0:T(8,128)(2,1)}, u32[]{:S(2)}) copy-start(bf16[256,2048]{1,0:T(8,128)(2,1)} %param.29) | copy-start | bytes 3145732
  6.5 203.9 %reduce-scatter.3.cloned.1.call-start = ((), (), s32[]{:S(2)}) async-start(), calls=%async_computation.2 | async-start | bytes 1966080 | tf_op jit(solution)/shard_map/reduce_scatter | solution.py:231
  78.7 96.8 %copy-start.13 = (f32[128]{0:T(128)S(1)}, f32[128]{0:T(128)}, u32[]{:S(2)}) copy-start(f32[128]{0:T(128)} %param.28) | copy-start | bytes 1540
  81.1 129.4 %copy-start.1 = (bf16[96,2048]{1,0:T(8,128)(2,1)S(1)}, bf16[96,2048]{1,0:T(8,128)(2,1)}, u32[]{:S(2)}) copy-start(bf16[96,2048]{1,0:T(8,128)(2,1)} %param.19) | copy-start | bytes 1179652
  81.1 130.6 %copy-start.12 = (f32[2048]{0:T(1024)S(1)}, f32[2048]{0:T(1024)}, u32[]{:S(2)}) copy-start(f32[2048]{0:T(1024)} %param.30) | copy-start | bytes 24580
  81.1 133.9 %copy-start.3 = (bf16[1408,256]{1,0:T(8,128)(2,1)S(1)}, bf16[1408,256]{1,0:T(8,128)(2,1)}, u32[]{:S(2)}) copy-start(bf16[1408,256]{1,0:T(8,128)(2,1)} %param.33) | copy-start | bytes 2162692
  124.3 6.8 %collective-permute-start = (bf16[2,128,128]{2,1,0:T(8,128)(2,1)S(1)}, bf16[2,128,128]{2,1,0:T(8,128)(2,1)S(1)}, u32[]{:S(2)}, u32[]{:S(2)}) collective-permute-start(bf16[2,128,128]{2,1,0:T(8,128)(2,1)S(1)} %fusion.155), channel_id=1, source_target_pairs={{0,4},{4,8},{8,12},{12,16},{16,20},{20,24},{24,28},{1,5},{5,9},{9,... | collective-permute-start | bytes 196616 | tf_op jit(solution)/shard_map/while/body/eval_jaxpr/ppermute | solution.py:15
  131.4 6.2 %collective-permute-start = (bf16[2,128,128]{2,1,0:T(8,128)(2,1)S(1)}, bf16[2,128,128]{2,1,0:T(8,128)(2,1)S(1)}, u32[]{:S(2)}, u32[]{:S(2)}) collective-permute-start(bf16[2,128,128]{2,1,0:T(8,128)(2,1)S(1)} %fusion.155), channel_id=1, source_target_pairs={{0,4},{4,8},{8,12},{12,16},{16,20},{20,24},{24,28},{1,5},{5,9},{9,... | collective-permute-start | bytes 196616 | tf_op jit(solution)/shard_map/while/body/eval_jaxpr/ppermute | solution.py:15
  137.9 6.2 %collective-permute-start = (bf16[2,128,128]{2,1,0:T(8,128)(2,1)S(1)}, bf16[2,128,128]{2,1,0:T(8,128)(2,1)S(1)}, u32[]{:S(2)}, u32[]{:S(2)}) collective-permute-start(bf16[2,128,128]{2,1,0:T(8,128)(2,1)S(1)} %fusion.155), channel_id=1, source_target_pairs={{0,4},{4,8},{8,12},{12,16},{16,20},{20,24},{24,28},{1,5},{5,9},{9,... | collective-permute-start | bytes 196616 | tf_op jit(solution)/shard_map/while/body/eval_jaxpr/ppermute | solution.py:15
  144.4 7.1 %collective-permute-start = (bf16[2,128,128]{2,1,0:T(8,128)(2,1)S(1)}, bf16[2,128,128]{2,1,0:T(8,128)(2,1)S(1)}, u32[]{:S(2)}, u32[]{:S(2)}) collective-permute-start(bf16[2,128,128]{2,1,0:T(8,128)(2,1)S(1)} %fusion.155), channel_id=1, source_target_pairs={{0,4},{4,8},{8,12},{12,16},{16,20},{20,24},{24,28},{1,5},{5,9},{9,... | collective-permute-start | bytes 196616 | tf_op jit(solution)/shard_map/while/body/eval_jaxpr/ppermute | solution.py:15
  151.8 7.1 %collective-permute-start = (bf16[2,128,128]{2,1,0:T(8,128)(2,1)S(1)}, bf16[2,128,128]{2,1,0:T(8,128)(2,1)S(1)}, u32[]{:S(2)}, u32[]{:S(2)}) collective-permute-start(bf16[2,128,128]{2,1,0:T(8,128)(2,1)S(1)} %fusion.155), channel_id=1, source_target_pairs={{0,4},{4,8},{8,12},{12,16},{16,20},{20,24},{24,28},{1,5},{5,9},{9,... | collective-permute-start | bytes 196616 | tf_op jit(solution)/shard_map/while/body/eval_jaxpr/ppermute | solution.py:15
  159.1 7.4 %collective-permute-start = (bf16[2,128,128]{2,1,0:T(8,128)(2,1)S(1)}, bf16[2,128,128]{2,1,0:T(8,128)(2,1)S(1)}, u32[]{:S(2)}, u32[]{:S(2)}) collective-permute-start(bf16[2,128,128]{2,1,0:T(8,128)(2,1)S(1)} %fusion.155), channel_id=1, source_target_pairs={{0,4},{4,8},{8,12},{12,16},{16,20},{20,24},{24,28},{1,5},{5,9},{9,... | collective-permute-start | bytes 196616 | tf_op jit(solution)/shard_map/while/body/eval_jaxpr/ppermute | solution.py:15
  166.8 7.0 %collective-permute-start = (bf16[2,128,128]{2,1,0:T(8,128)(2,1)S(1)}, bf16[2,128,128]{2,1,0:T(8,128)(2,1)S(1)}, u32[]{:S(2)}, u32[]{:S(2)}) collective-permute-start(bf16[2,128,128]{2,1,0:T(8,128)(2,1)S(1)} %fusion.155), channel_id=1, source_target_pairs={{0,4},{4,8},{8,12},{12,16},{16,20},{20,24},{24,28},{1,5},{5,9},{9,... | collective-permute-start | bytes 196616 | tf_op jit(solution)/shard_map/while/body/eval_jaxpr/ppermute | solution.py:15
  178.5 268.5 %all-gather.4.cloned.1.call-start = ((), (), s32[]{:S(2)}) async-start(), calls=%async_computation.3 | async-start | bytes 1966080 | tf_op jit(solution)/shard_map/all_gather | solution.py:239
  213.6 233.4 %all-gather.6.cloned.1.call-start = ((), (), s32[]{:S(2)}) async-start(), calls=%async_computation.4 | async-start | bytes 6488064 | tf_op jit(solution)/shard_map/all_gather | solution.py:170
  214.4 271.3 %all-gather.8.cloned.1.call-start = ((), (), s32[]{:S(2)}) async-start(), calls=%async_computation.5 | async-start | bytes 6488064 | tf_op jit(solution)/shard_map/all_gather | solution.py:171
  214.9 308.8 %reduce-scatter.5.cloned.1.call-start = ((), (), s32[]{:S(2)}) async-start(), calls=%async_computation.6 | async-start | bytes 1966080 | tf_op jit(solution)/shard_map/reduce_scatter | solution.py:241
  215.0 20.5 %collective-permute-start.1 = (bf16[1408,256]{1,0:T(8,128)(2,1)S(1)}, bf16[1408,256]{1,0:T(8,128)(2,1)S(1)}, u32[]{:S(2)}, u32[]{:S(2)}) collective-permute-start(bf16[1408,256]{1,0:T(8,128)(2,1)S(1)} %copy-done.3), channel_id=1, source_target_pairs={{0,4},{4,8},{8,12},{12,16},{16,20},{20,24},{24,28},{28,0},{1,5},{5... | collective-permute-start | bytes 2162696 | tf_op jit(solution)/shard_map/ppermute | solution.py:180
  235.5 27.2 %collective-permute-start.2 = (bf16[1408,256]{1,0:T(8,128)(2,1)S(1)}, bf16[1408,256]{1,0:T(8,128)(2,1)S(1)}, u32[]{:S(2)}, u32[]{:S(2)}) collective-permute-start(bf16[1408,256]{1,0:T(8,128)(2,1)S(1)} %collective-permute-done.1), channel_id=1, source_target_pairs={{0,4},{4,8},{8,12},{12,16},{16,20},{20,24},{24,28},{28,0},{1,5},{5... | collective-permute-start | bytes 2162696 | tf_op jit(solution)/shard_map/ppermute | solution.py:180
  262.6 0.9 copy-start.4
  263.5 30.2 %collective-permute-start.3 = (bf16[1408,256]{1,0:T(8,128)(2,1)S(1)}, bf16[1408,256]{1,0:T(8,128)(2,1)S(1)}, u32[]{:S(2)}, u32[]{:S(2)}) collective-permute-start(bf16[1408,256]{1,0:T(8,128)(2,1)S(1)} %collective-permute-done.2), channel_id=1, source_target_pairs={{0,4},{4,8},{8,12},{12,16},{16,20},{20,24},{24,28},{28,0},{1,5},{5... | collective-permute-start | bytes 2162696 | tf_op jit(solution)/shard_map/ppermute | solution.py:180
  293.7 0.9 copy-start.6
  294.6 35.0 %collective-permute-start.4 = (bf16[1408,256]{1,0:T(8,128)(2,1)S(1)}, bf16[1408,256]{1,0:T(8,128)(2,1)S(1)}, u32[]{:S(2)}, u32[]{:S(2)}) collective-permute-start(bf16[1408,256]{1,0:T(8,128)(2,1)S(1)} %collective-permute-done.3), channel_id=1, source_target_pairs={{0,4},{4,8},{8,12},{12,16},{16,20},{20,24},{24,28},{28,0},{1,5},{5... | collective-permute-start | bytes 2162696 | tf_op jit(solution)/shard_map/ppermute | solution.py:180
  329.6 0.9 copy-start.8
  330.5 35.1 %collective-permute-start.5 = (bf16[1408,256]{1,0:T(8,128)(2,1)S(1)}, bf16[1408,256]{1,0:T(8,128)(2,1)S(1)}, u32[]{:S(2)}, u32[]{:S(2)}) collective-permute-start(bf16[1408,256]{1,0:T(8,128)(2,1)S(1)} %collective-permute-done.4), channel_id=1, source_target_pairs={{0,4},{4,8},{8,12},{12,16},{16,20},{20,24},{24,28},{28,0},{1,5},{5... | collective-permute-start | bytes 2162696 | tf_op jit(solution)/shard_map/ppermute | solution.py:180
  365.6 0.9 copy-start.10
  366.5 23.5 %collective-permute-start.6 = (bf16[1408,256]{1,0:T(8,128)(2,1)S(1)}, bf16[1408,256]{1,0:T(8,128)(2,1)}, u32[]{:S(2)}, u32[]{:S(2)}) collective-permute-start(bf16[1408,256]{1,0:T(8,128)(2,1)S(1)} %collective-permute-done.5), channel_id=1, source_target_pairs={{0,4},{4,8},{8,12},{12,16},{16,20},{20,24},{24,28},{28,0},{1,5},{5... | collective-permute-start | bytes 2162696 | tf_op jit(solution)/shard_map/ppermute | solution.py:180
  390.1 32.3 %collective-permute-start.7 = (bf16[1408,256]{1,0:T(8,128)(2,1)}, bf16[1408,256]{1,0:T(8,128)(2,1)}, u32[]{:S(2)}, u32[]{:S(2)}) collective-permute-start(bf16[1408,256]{1,0:T(8,128)(2,1)} %collective-permute-done.6), channel_id=1, source_target_pairs={{0,4},{4,8},{8,12},{12,16},{16,20},{20,24},{24,28},{28,0},{1,5},{5... | collective-permute-start | bytes 2162696 | tf_op jit(solution)/shard_map/ppermute | solution.py:180
  390.1 51.2 %copy-start.11 = (bf16[1408,256]{1,0:T(8,128)(2,1)S(1)}, bf16[1408,256]{1,0:T(8,128)(2,1)}, u32[]{:S(2)}) copy-start(bf16[1408,256]{1,0:T(8,128)(2,1)} %copy-done.10) | copy-start | bytes 2162692
  390.1 52.2 %copy-start.9 = (bf16[1408,256]{1,0:T(8,128)(2,1)S(1)}, bf16[1408,256]{1,0:T(8,128)(2,1)}, u32[]{:S(2)}) copy-start(bf16[1408,256]{1,0:T(8,128)(2,1)} %copy-done.8) | copy-start | bytes 2162692
  390.1 53.1 %copy-start.7 = (bf16[1408,256]{1,0:T(8,128)(2,1)S(1)}, bf16[1408,256]{1,0:T(8,128)(2,1)}, u32[]{:S(2)}) copy-start(bf16[1408,256]{1,0:T(8,128)(2,1)} %copy-done.6) | copy-start | bytes 2162692
  390.1 54.1 %copy-start.5 = (bf16[1408,256]{1,0:T(8,128)(2,1)S(1)}, bf16[1408,256]{1,0:T(8,128)(2,1)}, u32[]{:S(2)}) copy-start(bf16[1408,256]{1,0:T(8,128)(2,1)} %copy-done.4) | copy-start | bytes 2162692
  454.1 69.6 %copy-start.2 = (bf16[96,2048]{1,0:T(8,128)(2,1)S(1)}, bf16[96,2048]{1,0:T(8,128)(2,1)}, u32[]{:S(2)}) copy-start(bf16[96,2048]{1,0:T(8,128)(2,1)} %reduce-scatter.3.cloned.1.call-done) | copy-start | bytes 1179652
Sparse Core Ops, SparseCore 0:
  178.6 31.7 reduce-scatter.2
  213.7 19.6 all-gather.3
  235.6 133.4 all-gather.5
  371.1 114.5 all-gather.7
  497.5 26.1 reduce-scatter.4
